TPU v7x, 32 devices: a whole 2x2x4 slice. The times are simulated.
32 devices in a mesh: grp: 2 (over y), ep: 4 (over z), tp: 4 (over x, core).
Axes of the slice: x: 2, y: 2, z: 4, core: 2. Of those that a mesh axis runs over, the one named last changes fastest.
Arguments:
- tokens: bfloat16 [4096, 2048], P(('grp', 'ep', 'tp')), parts along dimension 0, may hold values from -6 to 6
- norm_gain: float32 [2048], replicated, may hold values from 0.1 to 1.9
- route_ids: int32 [4096, 2], P(('grp', 'ep', 'tp')), parts along dimension 0, may hold values from 0 to 15, all different within a row; in each aligned block of 128 rows (0 to 127, 128 to 255, ...) at most 24 rows name the same one
- route_weights: float32 [4096, 2], P(('grp', 'ep', 'tp')), parts along dimension 0, may hold values from 0.1 to 0.9
- w_gate: bfloat16 [16, 2048, 512], P(('ep', 'tp')), may hold values from -0.125 to 0.125
- w_up: bfloat16 [16, 2048, 512], P(('ep', 'tp')), may hold values from -0.125 to 0.125
- w_down: bfloat16 [16, 512, 2048], P(('ep', 'tp')), may hold values from -0.25 to 0.25
Outputs:
- mixed: bfloat16 [4096, 2048], P(('grp', 'ep', 'tp')), parts along dimension 0
There are 2 independent parts, one for each index of `grp`. A program takes and returns all parts, laid end to end along the dimension named above; an argument that names none is the same for every part. Nothing has to cross between parts.
Inputs may be any that keep to these rules, and one draw needn't show every extreme that they name: `route_ids`: each token names 2 different experts. Among the tokens of one device (aligned blocks of 128 tokens) no expert is named more than 24 times, a bound that some block reaches.
All inputs are finite; a program needn't handle non-finite values.
Results may differ from a plain program's by a relative error of at most 0.0071.
Values may be sent and summed in bfloat16 or wider, within the bound.
A program may use at most 64 MiB of HBM per device.

v0:
```python
import jax
import jax.numpy as jnp
from jax import lax
from jax.sharding import PartitionSpec as P


def on_device(tokens, norm_gain, route_ids, route_weights, w_gate, w_up, w_down):
    tok_rows, model_width = tokens.shape
    top_count = route_ids.shape[1]
    ep_count = lax.axis_size("ep")
    tp_count = lax.axis_size("tp")
    experts = ep_count * tp_count
    capacity = 3 * tok_rows * top_count // (2 * experts)
    values = tokens.astype(jnp.float32)
    normed = (
        values * lax.rsqrt(jnp.mean(values * values, axis=-1, keepdims=True) + 1e-06) * norm_gain
    ).astype(jnp.bfloat16)
    flat_ids = route_ids.reshape(-1)
    onehot = (flat_ids[:, None] == jnp.arange(experts, dtype=jnp.int32)[None, :]).astype(jnp.int32)
    slot_index = jnp.sum((jnp.cumsum(onehot, axis=0) - onehot) * onehot, axis=-1)
    token_of = jnp.arange(tok_rows * top_count, dtype=jnp.int32) // top_count
    buffer = jnp.zeros((experts, capacity, model_width), jnp.bfloat16)
    buffer = buffer.at[flat_ids, slot_index].set(normed[token_of])
    received = lax.all_to_all(buffer, ("ep", "tp"), split_axis=0, concat_axis=0, tiled=True)
    flat_rows = received.reshape(-1, model_width)
    gate_act = jnp.dot(flat_rows, w_gate[0], preferred_element_type=jnp.float32)
    up_act = jnp.dot(flat_rows, w_up[0], preferred_element_type=jnp.float32)
    hidden = (jax.nn.silu(gate_act) * up_act).astype(jnp.bfloat16)
    result = jnp.dot(hidden, w_down[0], preferred_element_type=jnp.float32).astype(jnp.bfloat16)
    returned = lax.all_to_all(
        result.reshape(received.shape), ("ep", "tp"), split_axis=0, concat_axis=0, tiled=True
    )
    picked = (
        returned[flat_ids, slot_index].reshape(tok_rows, top_count, model_width).astype(jnp.float32)
    )
    return jnp.sum(picked * route_weights[:, :, None], axis=1).astype(jnp.bfloat16)


def solution(mesh):
    return jax.shard_map(
        on_device,
        mesh=mesh,
        in_specs=(
            P(("grp", "ep", "tp"), None),
            P(),
            P(("grp", "ep", "tp"), None),
            P(("grp", "ep", "tp"), None),
            P(("ep", "tp"), None, None),
            P(("ep", "tp"), None, None),
            P(("ep", "tp"), None, None),
        ),
        out_specs=P(("grp", "ep", "tp"), None),
        check_vma=False,
    )
```

profile of v0, /device:TPU:11, one launch (start us, length us, event | category | flops | bytes accessed | tf_op | source)
XLA Modules:
  0.0 156.8 jit_solution(10901765160997341917)
XLA Ops:
  0.0 0.0 copy-start
  0.0 0.9 copy.9
  0.9 0.1 eq.29
  1.1 0.1 eq.25
  1.2 0.1 reshape.123
  1.4 0.6 reduce-window.6
  2.0 0.2 slice_reduce_fusion
  2.2 1.2 fusion.11
  3.5 0.1 fusion.24
  3.6 1.2 fusion.13
  4.8 2.3 %gather_fusion = bf16[256,2048]{1,0:T(8,128)(2,1)} fusion(bf16[128,2048]{1,0:T(8,128)(2,1)S(1)} %fusion.13, s32[1024]{0:T(1024)S(1)} %pad_clamp_fusion), kind=kCustom, calls=%fused_computation | custom fusion | bytes 2098176 | tf_op jit(solution)/shard_map/gather | solution.py:23
  7.1 0.0 copy-start.1
  7.1 1.3 broadcast_in_dim.2
  8.5 0.1 copy-done.1
  8.6 44.4 %scatter_fusion = bf16[16,24,2048]{2,1,0:T(8,128)(2,1)} fusion(bf16[16,24,2048]{2,1,0:T(8,128)(2,1)} %broadcast_in_dim.2, s32[256]{0:T(256)S(1)} %bitcast.43, bf16[256,2048]{1,0:T(8,128)(2,1)S(1)} %copy-done.1), kind=kCustom, calls=%fused_computation.2 | custom fusion | bytes 3147776 | tf_op jit(solution)/shard_map/scatter | solution.py:23
  53.0 0.0 copy-start.4
  53.1 42.9 %all_to_all.10 = bf16[16,24,2048]{2,1,0:T(8,128)(2,1)S(1)} all-to-all(bf16[16,24,2048]{2,1,0:T(8,128)(2,1)} %scatter_fusion), channel_id=1, replica_groups=mesh['grp'=2,'ep'=4,'tp'=4] {'ep','tp'}, dimensions={0} | all-to-all | bytes 3145728 | tf_op jit(solution)/shard_map/all_to_all | solution.py:24
  95.9 0.0 copy-start.2
  95.9 1.1 copy-done.2
  97.1 0.0 copy-done.4
  97.1 1.0 fusion.3
  98.0 0.0 copy-done
  98.0 5.2 %convolution_convert_fusion = bf16[384,2048]{1,0:T(8,128)(2,1)} fusion(bf16[1,512,2048]{2,1,0:T(8,128)(2,1)S(1)} %copy-done, bf16[384,2048]{1,0:T(8,128)(2,1)} %bitcast.46, bf16[1,2048,512]{2,1,0:T(8,128)(2,1)} %param.12, f32[384,512]{1,0:T(8,128)S(1)} %fusion.3), kind=kOutput, calls=%fused_computation.3 | convolution fusion | flops 1612578816 | bytes 8126464 | tf_op jit(solution)/shard_map/dot_general | solution.py:29
  103.2 0.0 copy-start.3
  103.2 5.1 %all-to-all-start.1 = ((bf16[16,24,2048]{2,1,0:T(8,128)(2,1)}), bf16[16,24,2048]{2,1,0:T(8,128)(2,1)}, u32[]{:S(2)}, u32[]{:S(2)}) async-start(bf16[16,24,2048]{2,1,0:T(8,128)(2,1)} %bitcast.44), calls=%async_computation.1 | async-start | bytes 3145728 | tf_op jit(solution)/shard_map/all_to_all | solution.py:30
  108.3 0.0 copy-done.3
  108.3 0.1 copy.13
  108.4 36.2 %all-to-all-done.1 = bf16[16,24,2048]{2,1,0:T(8,128)(2,1)} async-done(((bf16[16,24,2048]{2,1,0:T(8,128)(2,1)}), bf16[16,24,2048]{2,1,0:T(8,128)(2,1)}, u32[]{:S(2)}, u32[]{:S(2)}) %all-to-all-start.1) | async-done | bytes 1572896 | tf_op jit(solution)/shard_map/all_to_all | solution.py:30
  144.6 4.3 %gather_fusion.1 = bf16[256,2048]{1,0:T(8,128)(2,1)S(1)} fusion(bf16[16,24,2048]{2,1,0:T(8,128)(2,1)} %all-to-all-done.1, s32[256]{0:T(256)S(1)} %bitcast.42), kind=kCustom, calls=%fused_computation.1 | custom fusion | bytes 2099200 | tf_op jit(solution)/shard_map/gather | solution.py:34
  148.8 2.4 %reshape.127 = f32[128,2,2048]{2,1,0:T(2,128)} reshape(bf16[256,2048]{1,0:T(8,128)(2,1)S(1)} %gather_fusion.1) | data formatting | bytes 3145728 | tf_op jit(solution)/shard_map/convert_element_type | solution.py:34
  151.2 5.6 %multiply_reduce_fusion = bf16[128,2048]{1,0:T(8,128)(2,1)} fusion(f32[128,2,2048]{2,1,0:T(2,128)} %reshape.127, f32[128,2]{1,0:T(8,128)S(1)} %copy.13), kind=kLoop, calls=%fused_computation.9 | loop fusion | flops 786432 | bytes 2622464 | tf_op jit(solution)/shard_map/reduce_sum | solution.py:36
  (7 shorter events, 0.1 us)
Async XLA Ops:
  0.0 98.0 %copy-start = (bf16[1,512,2048]{2,1,0:T(8,128)(2,1)S(1)}, bf16[1,512,2048]{2,1,0:T(8,128)(2,1)}, u32[]{:S(2)}) copy-start(bf16[1,512,2048]{2,1,0:T(8,128)(2,1)} %param.13) | copy-start | bytes 6291460
  7.1 1.5 copy-start.1
  53.0 44.0 %copy-start.4 = (bf16[1,2048,512]{2,1,0:T(8,128)(2,1)S(1)}, bf16[1,2048,512]{2,1,0:T(8,128)(2,1)}, u32[]{:S(2)}) copy-start(bf16[1,2048,512]{2,1,0:T(8,128)(2,1)} %param.11) | copy-start | bytes 6291460
  95.9 1.1 copy-start.2
  103.2 5.1 %copy-start.3 = (f32[128,2]{0,1:T(2,128)S(1)}, f32[128,2]{0,1:T(2,128)}, u32[]{:S(2)}) copy-start(f32[128,2]{0,1:T(2,128)} %param.10) | copy-start | bytes 3076
  103.2 41.4 %all-to-all-start.1 = ((bf16[16,24,2048]{2,1,0:T(8,128)(2,1)}), bf16[16,24,2048]{2,1,0:T(8,128)(2,1)}, u32[]{:S(2)}, u32[]{:S(2)}) async-start(bf16[16,24,2048]{2,1,0:T(8,128)(2,1)} %bitcast.44), calls=%async_computation.1 | async-start | bytes 3145728 | tf_op jit(solution)/shard_map/all_to_all | solution.py:30
where the time goes:
time: 159 us; the launch traced here: 157 us
  local copies, waits for them, and re-layouts  57.7 us (36%)
  blocking collectives  42.9 us (27%)
  waiting for transfers between devices  36.2 us (23%)
  other arithmetic  8.81 us (6%)
  matrix products  6.12 us (4%)
  starting transfers between devices  5.09 us (3%)
    scatter x1, local copies, waits for them, and re-layouts, on_device(): buffer = buffer.at[flat_ids, slot_index].set(normed[token_of])  44.4 us
    all_to_all x1, blocking collectives, on_device(): lax.all_to_all(buffer, ('ep', 'tp'), split_axis=0, concat_axis=0, tiled=T...  42.9 us
    all_to_all x1, waiting for transfers between devices, on_device(): lax.all_to_all(result.reshape(received.shape), ('ep', 'tp'), split_axis=0...  36.2 us
    reduce_sum x1, other arithmetic, on_device(): jnp.sum(picked * route_weights[:, :, None], axis=1).astype(jnp.bfloat16)  5.59 us
    dot_general x1, matrix products, on_device(): jnp.dot(hidden, w_down[0], preferred_element_type=jnp.float32)  5.15 us
    all_to_all x1, starting transfers between devices, on_device(): lax.all_to_all(result.reshape(received.shape), ('ep', 'tp'), split_axis=0...  5.09 us
    gather x1, local copies, waits for them, and re-layouts, on_device(): returned[flat_ids, slot_index].reshape(tok_rows, top_count, model_width)  4.26 us
  transfers between devices with their start and end apart: 1, of which 1 were waited for; matrix products, arithmetic and copies ran while one was open for 0% of the time, Pallas kernels for 0%

commit v1 on v0

--- a/solution.py
+++ b/solution.py
@@ -1,10 +1,16 @@
+import functools
+
 import jax
 import jax.numpy as jnp
 from jax import lax
+from jax.experimental import pallas as pl
+from jax.experimental.pallas import tpu as pltpu
 from jax.sharding import PartitionSpec as P
 
-
-def on_device(tokens, norm_gain, route_ids, route_weights, w_gate, w_up, w_down):
+MESH = pl.DeviceIdType.MESH
+
+
+def plain(tokens, norm_gain, route_ids, route_weights, w_gate, w_up, w_down):
     tok_rows, model_width = tokens.shape
     top_count = route_ids.shape[1]
     ep_count = lax.axis_size("ep")
@@ -36,7 +42,190 @@
     return jnp.sum(picked * route_weights[:, :, None], axis=1).astype(jnp.bfloat16)
 
 
+def flipped(index, bits):
+    bit = 1
+    while bit <= bits:
+        if bits & bit:
+            index = index + (1 - 2 * ((index // bit) % 2)) * bit
+        bit *= 2
+    return index
+
+
+def kernel(
+    ep_count, tp_count, cap,
+    x_ref, gain_ref, ids_ref, wts_ref, wg_hbm, wu_hbm, wd_hbm, out_ref,
+    send, recv, res, back, wg, wu, wd, comb_hi, comb_lo, acc,
+    w_sem, send_sem, recv_sem, ret_sem, back_sem,
+):
+    ep, tp, grp = lax.axis_index("ep"), lax.axis_index("tp"), lax.axis_index("grp")
+    rows, width = x_ref.shape
+    top = ids_ref.shape[1]
+    experts = ep_count * tp_count
+    me = ep * tp_count + tp
+
+    def peer(g):
+        return (grp, flipped(ep, g // tp_count), flipped(tp, g % tp_count))
+
+    barrier = pltpu.get_barrier_semaphore()
+    for g in range(1, experts):
+        pl.semaphore_signal(barrier, inc=1, device_id=peer(g), device_id_type=MESH)
+    loads = [
+        pltpu.make_async_copy(src.at[0], dst, w_sem.at[i])
+        for i, (src, dst) in enumerate(((wg_hbm, wg), (wu_hbm, wu), (wd_hbm, wd)))
+    ]
+    for load in loads:
+        load.start()
+
+    down = lax.broadcasted_iota(jnp.int32, (rows, rows), 0)
+    across = lax.broadcasted_iota(jnp.int32, (rows, rows), 1)
+
+    def as_row(column):
+        return jnp.sum(jnp.where(down == across, column, 0), axis=0, keepdims=True)
+
+    expert_of = lax.broadcasted_iota(jnp.int32, (experts, rows), 0) ^ me
+    ids, wts = ids_ref[...], wts_ref[...]
+    named = jnp.zeros((experts, rows), jnp.float32)
+    weight = jnp.zeros((experts, rows), jnp.float32)
+    for k in range(top):
+        match = as_row(ids[:, k:k + 1]) == expert_of
+        named = named + jnp.where(match, 1.0, 0.0)
+        weight = weight + jnp.where(match, as_row(wts[:, k:k + 1]), 0.0)
+    earlier = jnp.where(down < across, 1.0, 0.0).astype(jnp.bfloat16)
+    rank = jnp.dot(named.astype(jnp.bfloat16), earlier, preferred_element_type=jnp.float32)
+    rank = jnp.where(named > 0.5, rank, -1.0)
+    slot = lax.broadcasted_iota(jnp.int32, (experts, cap, rows), 1).astype(jnp.float32)
+    taken = rank[:, None, :] == slot
+    pick = jnp.where(taken, 1.0, 0.0).reshape(experts * cap, rows).astype(jnp.bfloat16)
+    share = jnp.where(taken, weight[:, None, :], 0.0).reshape(experts * cap, rows)
+    share_hi = share.astype(jnp.bfloat16)
+    comb_hi[...] = share_hi
+    comb_lo[...] = (share - share_hi.astype(jnp.float32)).astype(jnp.bfloat16)
+
+    values = x_ref[...].astype(jnp.float32)
+    normed = (
+        values
+        * lax.rsqrt(jnp.mean(values * values, axis=-1, keepdims=True) + 1e-06)
+        * gain_ref[...]
+    ).astype(jnp.bfloat16)
+
+    pl.semaphore_wait(barrier, experts - 1)
+    out_copies, ret_copies = {}, {}
+
+    def start_group(r):
+        for g in range(r * tp_count, (r + 1) * tp_count):
+            if g:
+                out_copies[g].start()
+
+    order = list(range(ep_count - 1, -1, -1))
+    for r in order:
+        base = r * tp_count
+        packed = jnp.dot(
+            pick[base * cap:(base + tp_count) * cap], normed, preferred_element_type=jnp.float32
+        ).astype(jnp.bfloat16).reshape(tp_count, cap, width)
+        for j in range(tp_count):
+            g = base + j
+            if g == 0:
+                recv[0] = packed[0]
+            else:
+                send[g] = packed[j]
+                out_copies[g] = pltpu.make_async_remote_copy(
+                    src_ref=send.at[g], dst_ref=recv.at[g],
+                    send_sem=send_sem.at[g], recv_sem=recv_sem.at[g],
+                    device_id=peer(g), device_id_type=MESH,
+                )
+        start_group(r)
+    for load in loads:
+        load.wait()
+
+    for r in order:
+        base = r * tp_count
+        for g in range(base, base + tp_count):
+            if g:
+                out_copies[g].wait_recv()
+        block = recv[base:base + tp_count].reshape(tp_count * cap, width)
+        gate_act = jnp.dot(block, wg[...], preferred_element_type=jnp.float32)
+        up_act = jnp.dot(block, wu[...], preferred_element_type=jnp.float32)
+        hidden = (gate_act / (1.0 + jnp.exp(-gate_act)) * up_act).astype(jnp.bfloat16)
+        result = jnp.dot(hidden, wd[...], preferred_element_type=jnp.float32)
+        result = result.astype(jnp.bfloat16).reshape(tp_count, cap, width)
+        for j in range(tp_count):
+            g = base + j
+            if g == 0:
+                back[0] = result[0]
+            else:
+                res[g] = result[j]
+                ret_copies[g] = pltpu.make_async_remote_copy(
+                    src_ref=res.at[g], dst_ref=back.at[g],
+                    send_sem=ret_sem.at[g], recv_sem=back_sem.at[g],
+                    device_id=peer(g), device_id_type=MESH,
+                )
+                ret_copies[g].start()
+
+    for step, r in enumerate(order):
+        base = r * tp_count
+        for g in range(base, base + tp_count):
+            if g:
+                ret_copies[g].wait_recv()
+        block = back[base:base + tp_count].reshape(tp_count * cap, width)
+        part = sum(
+            lax.dot_general(
+                comb[base * cap:(base + tp_count) * cap, :], block,
+                (((0,), (0,)), ((), ())), preferred_element_type=jnp.float32,
+            )
+            for comb in (comb_hi, comb_lo)
+        )
+        if step == 0:
+            acc[...] = part
+        elif step < ep_count - 1:
+            acc[...] += part
+        else:
+            out_ref[...] = (acc[...] + part).astype(out_ref.dtype)
+    for g in range(1, experts):
+        out_copies[g].wait_send()
+        ret_copies[g].wait_send()
+
+
+def fused(ep_count, tp_count, tokens, norm_gain, route_ids, route_weights, w_gate, w_up, w_down):
+    rows, width = tokens.shape
+    hidden = w_gate.shape[2]
+    experts = ep_count * tp_count
+    cap = 3 * rows * route_ids.shape[1] // (2 * experts)
+    vmem = pl.BlockSpec(memory_space=pltpu.VMEM)
+    hbm = pl.BlockSpec(memory_space=pl.ANY)
+    slots = pltpu.VMEM((experts, cap, width), jnp.bfloat16)
+    sems = pltpu.SemaphoreType.DMA((experts,))
+    return pl.pallas_call(
+        functools.partial(kernel, ep_count, tp_count, cap),
+        out_shape=jax.ShapeDtypeStruct((rows, width), tokens.dtype),
+        in_specs=[vmem] * 4 + [hbm] * 3,
+        out_specs=vmem,
+        scratch_shapes=[
+            slots, slots, slots, slots,
+            pltpu.VMEM((width, hidden), jnp.bfloat16),
+            pltpu.VMEM((width, hidden), jnp.bfloat16),
+            pltpu.VMEM((hidden, width), jnp.bfloat16),
+            pltpu.VMEM((experts * cap, rows), jnp.bfloat16),
+            pltpu.VMEM((experts * cap, rows), jnp.bfloat16),
+            pltpu.VMEM((rows, width), jnp.float32),
+            pltpu.SemaphoreType.DMA((3,)),
+            sems, sems, sems, sems,
+        ],
+        compiler_params=pltpu.CompilerParams(
+            collective_id=0, has_side_effects=True, vmem_limit_bytes=56 * 1024 * 1024
+        ),
+    )(tokens, norm_gain.reshape(1, width), route_ids, route_weights, w_gate, w_up, w_down)
+
+
 def solution(mesh):
+    ep_count, tp_count = mesh.shape["ep"], mesh.shape["tp"]
+
+    def on_device(*args):
+        rows, experts = args[0].shape[0], ep_count * tp_count
+        cap = 3 * rows * args[2].shape[1] // (2 * experts)
+        if cap % 8 or rows % 128 or experts & (experts - 1) or experts > 32:
+            return plain(*args)
+        return fused(ep_count, tp_count, *args)
+
     return jax.shard_map(
         on_device,
         mesh=mesh,

time: 159 us -> 85.6 us (0.54)
  the two profiles are of different devices: /device:TPU:11 before, /device:TPU:0 now
where the time goes in v1:
time: 85.6 us; the launch traced here: 85.4 us
  Pallas kernels  80.7 us (94%)
  local copies, waits for them, and re-layouts  4.7 us (5%)
    pallas_call x1, Pallas kernels, fused(): pl.pallas_call(functools.partial(kernel, ep_count, tp_count, cap), out_sh...  80.7 us
    unnamed x3, local copies, waits for them, and re-layouts  4.7 us

profile of v1, /device:TPU:0, one launch (start us, length us, event | category | flops | bytes accessed | tf_op | source)
XLA Modules:
  0.0 85.4 jit_solution(10820651480705444198)
XLA Ops:
  0.0 1.4 %copy.8.ids_ref = s32[128,2]{1,0:T(8,128)} copy(s32[128,2]{0,1:T(2,128)} %param.9) | data formatting | bytes 2048 | tf_op args[2]
  1.4 1.4 %copy.9.wts_ref = f32[128,2]{1,0:T(8,128)} copy(f32[128,2]{0,1:T(2,128)} %param.10) | data formatting | bytes 2048 | tf_op args[3]
  2.8 80.7 %shard_map.73 = bf16[128,2048]{1,0:T(8,128)(2,1)} custom-call(bf16[128,2048]{1,0:T(8,128)(2,1)} %x_ref.1, f32[1,2048]{1,0:T(1,128)} %bitcast.1, s32[128,2]{1,0:T(8,128)} %copy.8.ids_ref, f32[128,2]{1,0:T(8,128)} %copy.9.wts_ref, bf16[1,2048,512]{2,1,0:T(8,128)(2,1)} %wg_hbm.1, bf16[1,2048,512]{2,1,0:T(8,128)(2,1)} %wu_hbm.1, bf16[1,512,2048]{2,1,0:T(8,128)(2,1)} %wd_hbm.1), custom_call_target="tpu_custom_call" | custom-call | tf_op jit(solution)/shard_map/pallas_call | solution.py:197
  83.5 1.9 %copy.11 = bf16[128,2048]{1,0:T(8,128)(2,1)} copy(bf16[128,2048]{1,0:T(8,128)(2,1)} %shard_map.73) | data formatting | bytes 1048576

commit v2 on v0

--- a/solution.py
+++ b/solution.py
@@ -1,10 +1,16 @@
+import functools
+
 import jax
 import jax.numpy as jnp
 from jax import lax
+from jax.experimental import pallas as pl
+from jax.experimental.pallas import tpu as pltpu
 from jax.sharding import PartitionSpec as P
 
-
-def on_device(tokens, norm_gain, route_ids, route_weights, w_gate, w_up, w_down):
+MESH = pl.DeviceIdType.MESH
+
+
+def plain(tokens, norm_gain, route_ids, route_weights, w_gate, w_up, w_down):
     tok_rows, model_width = tokens.shape
     top_count = route_ids.shape[1]
     ep_count = lax.axis_size("ep")
@@ -36,7 +42,368 @@
     return jnp.sum(picked * route_weights[:, :, None], axis=1).astype(jnp.bfloat16)
 
 
+def flipped(index, bits):
+    bit = 1
+    while bit <= bits:
+        if bits & bit:
+            index = index + (1 - 2 * ((index // bit) % 2)) * bit
+        bit *= 2
+    return index
+
+
+PIECES = 2
+
+
+def kernel(
+    ep_count, tp_count, cap,
+    x_ref, gain_ref, ids_ref, wts_ref, wg_hbm, wu_hbm, wd_hbm, out_ref,
+    normed, meta, share_hi, share_lo, nsend, nrecv, nres, nback,
+    rblock, rmeta, rpick, rshare_hi, rshare_lo, fsend, frecv, fres, rback, rsend, farback,
+    wg, wu, wd, acc,
+    w_sem, dense_s, dense_r, meta_s, meta_r, near_s, near_r, nret_s, nret_r,
+    far_s, far_r, fret_s, fret_r, final_s, final_r,
+):
+    ep, tp, grp = lax.axis_index("ep"), lax.axis_index("tp"), lax.axis_index("grp")
+    rows, width = x_ref.shape
+    part_w = width // PIECES
+    top = ids_ref.shape[1]
+    experts = ep_count * tp_count
+    near = 2 * tp_count
+    me = ep * tp_count + tp
+    boundary = (ep + ep // 2) % 2
+    wave_of_me = 1 - boundary
+    own_relay, other_relay = 1 + ep // 2, 2 - ep // 2
+    is_boundary, is_end = boundary == 1, boundary == 0
+
+    def at(plane, j):
+        return (grp, plane, flipped(tp, j))
+
+    def remote(src, dst, s_sem, r_sem, target):
+        return pltpu.make_async_remote_copy(
+            src_ref=src, dst_ref=dst, send_sem=s_sem, recv_sem=r_sem,
+            device_id=target, device_id_type=MESH,
+        )
+
+    barrier = pltpu.get_barrier_semaphore()
+    for g in range(1, experts):
+        pl.semaphore_signal(
+            barrier, inc=1, device_id=at(flipped(ep, g // tp_count), g % tp_count),
+            device_id_type=MESH,
+        )
+    loads = [
+        pltpu.make_async_copy(src.at[0], dst, w_sem.at[i])
+        for i, (src, dst) in enumerate(((wg_hbm, wg), (wu_hbm, wu), (wd_hbm, wd)))
+    ]
+    for load in loads:
+        load.start()
+
+    planes = [ep, flipped(ep, 1)]
+    dense = [
+        remote(normed.at[c], rblock.at[wave_of_me, c], dense_s.at[c], dense_r.at[wave_of_me, c],
+               at(other_relay, 0))
+        for c in range(PIECES)
+    ]
+    meta_copy = remote(meta, rmeta.at[wave_of_me], meta_s.at[0], meta_r.at[wave_of_me],
+                       at(other_relay, 0))
+    near_out = [
+        remote(nsend.at[g], nrecv.at[g], near_s.at[g], near_r.at[g],
+               at(planes[g // tp_count], g % tp_count))
+        for g in range(near)
+    ]
+    near_ret = [
+        remote(nres.at[g], nback.at[g], nret_s.at[g], nret_r.at[g],
+               at(planes[g // tp_count], g % tp_count))
+        for g in range(near)
+    ]
+    far_out, far_ret, final = {}, {}, {}
+    for v in range(2):
+        for c in range(PIECES):
+            for i in range(near):
+                far_out[v, c, i] = remote(
+                    fsend.at[v, c, i], frecv.at[v, c, i % tp_count], far_s.at[v, c, i],
+                    far_r.at[v, c, i % tp_count], at(planes[i // tp_count], i % tp_count))
+            for j in range(tp_count):
+                place = wave_of_me * tp_count + j
+                far_ret[v, c, j] = remote(
+                    fres.at[v, c, j], rback.at[v, c, place], fret_s.at[v, c, j],
+                    fret_r.at[v, c, place], at(own_relay, j))
+            final[v, c] = remote(rsend.at[v, c], farback.at[c], final_s.at[v, c], final_r.at[c],
+                                 at(flipped(ep, 3 - v), 0))
+
+    values = x_ref[...].astype(jnp.float32)
+    rows_normed = (
+        values
+        * lax.rsqrt(jnp.mean(values * values, axis=-1, keepdims=True) + 1e-06)
+        * gain_ref[...]
+    ).astype(jnp.bfloat16)
+    for c in range(PIECES):
+        normed[c] = rows_normed[:, c * part_w:(c + 1) * part_w]
+
+    down = lax.broadcasted_iota(jnp.int32, (rows, rows), 0)
+    across = lax.broadcasted_iota(jnp.int32, (rows, rows), 1)
+
+    def as_row(column):
+        return jnp.sum(jnp.where(down == across, column, 0), axis=0, keepdims=True)
+
+    expert_of = lax.broadcasted_iota(jnp.int32, (experts, rows), 0) ^ me
+    ids, wts = ids_ref[...], wts_ref[...]
+    named = jnp.zeros((experts, rows), jnp.float32)
+    weight = jnp.zeros((experts, rows), jnp.float32)
+    for k in range(top):
+        match = as_row(ids[:, k:k + 1]) == expert_of
+        named = named + jnp.where(match, 1.0, 0.0)
+        weight = weight + jnp.where(match, as_row(wts[:, k:k + 1]), 0.0)
+    earlier = jnp.where(down < across, 1.0, 0.0).astype(jnp.bfloat16)
+    rank = jnp.dot(named.astype(jnp.bfloat16), earlier, preferred_element_type=jnp.float32)
+    rank = jnp.where(named > 0.5, rank, -1.0)
+    meta[0:near] = rank[near:]
+    meta[near:] = weight[near:]
+
+    def onehots(rank, weight):
+        slot = lax.broadcasted_iota(jnp.int32, (near, cap, rows), 1).astype(jnp.float32)
+        taken = rank[:, None, :] == slot
+        pick = jnp.where(taken, 1.0, 0.0).reshape(near * cap, rows).astype(jnp.bfloat16)
+        share = jnp.where(taken, weight[:, None, :], 0.0).reshape(near * cap, rows)
+        high = share.astype(jnp.bfloat16)
+        return pick, high, (share - high.astype(jnp.float32)).astype(jnp.bfloat16)
+
+    pl.semaphore_wait(barrier, experts - 1)
+
+    @pl.when(is_boundary)
+    def _():
+        meta_copy.start()
+        for c in range(PIECES):
+            dense[c].start()
+
+    pick, high, low = onehots(rank[:near], weight[:near])
+    share_hi[...] = high
+    share_lo[...] = low
+
+    def pack_near(p):
+        packed = jnp.dot(
+            pick[p * tp_count * cap:(p + 1) * tp_count * cap], rows_normed,
+            preferred_element_type=jnp.float32,
+        ).astype(jnp.bfloat16).reshape(tp_count, cap, width)
+        for j in range(tp_count):
+            g = p * tp_count + j
+            if g:
+                nsend[g] = packed[j]
+            else:
+                nrecv[0] = packed[0]
+        for j in range(tp_count):
+            if p or j:
+                near_out[p * tp_count + j].start()
+
+    pack_near(1)
+
+    @pl.when(is_end)
+    def _():
+        meta_copy.start()
+        for c in range(PIECES):
+            dense[c].start()
+
+    pack_near(0)
+
+    def hidden_of(gate_act, up_act):
+        return (gate_act / (1.0 + jnp.exp(-gate_act)) * up_act).astype(jnp.bfloat16)
+
+    def dot(a, b):
+        return jnp.dot(a, b, preferred_element_type=jnp.float32)
+
+    def expert_near(p):
+        base = p * tp_count
+        for g in range(base, base + tp_count):
+            if g:
+                near_out[g].wait_recv()
+        block = nrecv[base:base + tp_count].reshape(tp_count * cap, width)
+        hidden = hidden_of(dot(block, wg[...]), dot(block, wu[...]))
+        result = dot(hidden, wd[...]).astype(jnp.bfloat16).reshape(tp_count, cap, width)
+        for j in range(tp_count):
+            if p or j:
+                nres[base + j] = result[j]
+            else:
+                nback[0] = result[0]
+        for j in range(tp_count):
+            if p or j:
+                near_ret[base + j].start()
+
+    def relay_out(v, c):
+        @pl.when(is_boundary)
+        def _():
+            if c == 0:
+                remote(meta, rmeta.at[v], meta_s.at[0], meta_r.at[v], at(other_relay, 0)).wait_recv()
+                ranks, weights = rmeta[v, 0:near], rmeta[v, near:]
+                if v == 0:
+                    ranks = jnp.concatenate([ranks[tp_count:], ranks[:tp_count]], axis=0)
+                    weights = jnp.concatenate([weights[tp_count:], weights[:tp_count]], axis=0)
+                rp, rh, rl = onehots(ranks, weights)
+                rpick[v] = rp
+                rshare_hi[v] = rh
+                rshare_lo[v] = rl
+            remote(normed.at[c], rblock.at[v, c], dense_s.at[c], dense_r.at[v, c],
+                   at(other_relay, 0)).wait_recv()
+            packed = dot(rpick[v], rblock[v, c]).astype(jnp.bfloat16).reshape(near, cap, part_w)
+            frecv[v, c, 0] = packed[0]
+            for i in range(1, near):
+                fsend[v, c, i] = packed[i]
+            for i in list(range(tp_count, near)) + list(range(1, tp_count)):
+                far_out[v, c, i].start()
+
+    def expert_far(v):
+        gate_act = up_act = None
+        for c in range(PIECES):
+            for j in range(1, tp_count):
+                far_out[v, c, j].wait_recv()
+
+            @pl.when(is_end)
+            def _():
+                far_out[v, c, tp_count].wait_recv()
+
+            block = frecv[v, c].reshape(tp_count * cap, part_w)
+            more_gate = dot(block, wg[c * part_w:(c + 1) * part_w])
+            more_up = dot(block, wu[c * part_w:(c + 1) * part_w])
+            gate_act = more_gate if c == 0 else gate_act + more_gate
+            up_act = more_up if c == 0 else up_act + more_up
+        hidden = hidden_of(gate_act, up_act)
+        for c in range(PIECES):
+            result = dot(hidden, wd[:, c * part_w:(c + 1) * part_w])
+            result = result.astype(jnp.bfloat16).reshape(tp_count, cap, part_w)
+            fres[v, c] = result
+            for j in range(1, tp_count):
+                far_ret[v, c, j].start()
+
+            @pl.when(is_end)
+            def _():
+                far_ret[v, c, 0].start()
+
+            @pl.when(is_boundary)
+            def _():
+                rback[v, c, 0] = fres[v, c, 0]
+
+    def combine(high, low, block):
+        total = None
+        for comb in (high, low):
+            term = lax.dot_general(
+                comb, block, (((0,), (0,)), ((), ())), preferred_element_type=jnp.float32
+            )
+            total = term if total is None else total + term
+        return total
+
+    def relay_back(v, c):
+        @pl.when(is_boundary)
+        def _():
+            for i in range(1, near):
+                remote(fres.at[v, c, 0], rback.at[v, c, i], fret_s.at[v, c, 0],
+                       fret_r.at[v, c, i], at(own_relay, 1)).wait_recv()
+            block = rback[v, c].reshape(near * cap, part_w)
+            rsend[v, c] = combine(rshare_hi[v], rshare_lo[v], block).astype(jnp.bfloat16)
+            final[v, c].start()
+
+    for load in loads:
+        load.wait()
+    expert_near(0)
+    relay_out(0, 0)
+    expert_near(1)
+    for c in range(1, PIECES):
+        relay_out(0, c)
+    relay_out(1, 0)
+    expert_far(0)
+    for c in range(1, PIECES):
+        relay_out(1, c)
+    relay_back(0, 0)
+    expert_far(1)
+    for c in range(1, PIECES):
+        relay_back(0, c)
+
+    for g in range(1, near):
+        near_ret[g].wait_recv()
+    acc[...] = combine(share_hi[...], share_lo[...], nback[...].reshape(near * cap, width))
+    for c in range(PIECES):
+        relay_back(1, c)
+    for c in range(PIECES):
+        final[0, c].wait_recv()
+        part = acc[:, c * part_w:(c + 1) * part_w] + farback[c].astype(jnp.float32)
+        out_ref[:, c * part_w:(c + 1) * part_w] = part.astype(out_ref.dtype)
+
+    meta_copy.wait_send()
+    for copy in dense + near_out[1:] + near_ret[1:]:
+        copy.wait_send()
+    for v in range(2):
+        for c in range(PIECES):
+            for j in range(1, tp_count):
+                far_ret[v, c, j].wait_send()
+
+    @pl.when(is_end)
+    def _():
+        for v in range(2):
+            for c in range(PIECES):
+                far_ret[v, c, 0].wait_send()
+
+    @pl.when(is_boundary)
+    def _():
+        for v in range(2):
+            for c in range(PIECES):
+                for i in range(1, near):
+                    far_out[v, c, i].wait_send()
+                final[v, c].wait_send()
+
+
+def fused(ep_count, tp_count, tokens, norm_gain, route_ids, route_weights, w_gate, w_up, w_down):
+    rows, width = tokens.shape
+    hidden = w_gate.shape[2]
+    experts = ep_count * tp_count
+    near = 2 * tp_count
+    cap = 3 * rows * route_ids.shape[1] // (2 * experts)
+    part_w = width // PIECES
+    vmem = pl.BlockSpec(memory_space=pltpu.VMEM)
+    hbm = pl.BlockSpec(memory_space=pl.ANY)
+
+    def b16(*shape):
+        return pltpu.VMEM(shape, jnp.bfloat16)
+
+    def sems(*shape):
+        return pltpu.SemaphoreType.DMA(shape)
+
+    return pl.pallas_call(
+        functools.partial(kernel, ep_count, tp_count, cap),
+        out_shape=jax.ShapeDtypeStruct((rows, width), tokens.dtype),
+        in_specs=[vmem] * 4 + [hbm] * 3,
+        out_specs=vmem,
+        scratch_shapes=[
+            b16(PIECES, rows, part_w), pltpu.VMEM((2 * near, rows), jnp.float32),
+            b16(near * cap, rows), b16(near * cap, rows),
+            *[b16(near, cap, width)] * 4,
+            b16(2, PIECES, rows, part_w), pltpu.VMEM((2, 2 * near, rows), jnp.float32),
+            *[b16(2, near * cap, rows)] * 3,
+            b16(2, PIECES, near, cap, part_w),
+            b16(2, PIECES, tp_count, cap, part_w),
+            b16(2, PIECES, tp_count, cap, part_w),
+            b16(2, PIECES, near, cap, part_w),
+            b16(2, PIECES, rows, part_w), b16(PIECES, rows, part_w),
+            b16(width, hidden), b16(width, hidden), b16(hidden, width),
+            pltpu.VMEM((rows, width), jnp.float32),
+            sems(3), sems(PIECES), sems(2, PIECES), sems(1), sems(2),
+            sems(near), sems(near), sems(near), sems(near),
+            sems(2, PIECES, near), sems(2, PIECES, tp_count),
+            sems(2, PIECES, tp_count), sems(2, PIECES, near),
+            sems(2, PIECES), sems(PIECES),
+        ],
+        compiler_params=pltpu.CompilerParams(
+            collective_id=0, has_side_effects=True, vmem_limit_bytes=56 * 1024 * 1024
+        ),
+    )(tokens, norm_gain.reshape(1, width), route_ids, route_weights, w_gate, w_up, w_down)
+
+
 def solution(mesh):
+    ep_count, tp_count = mesh.shape["ep"], mesh.shape["tp"]
+
+    def on_device(*args):
+        rows, experts = args[0].shape[0], ep_count * tp_count
+        cap = 3 * rows * args[2].shape[1] // (2 * experts)
+        if ep_count != 4 or tp_count != 4 or cap % 8 or rows % 128 or args[0].shape[1] % 256:
+            return plain(*args)
+        return fused(ep_count, tp_count, *args)
+
     return jax.shard_map(
         on_device,
         mesh=mesh,

time: 159 us -> 82.6 us (0.52)
  the two profiles are of different devices: /device:TPU:11 before, /device:TPU:0 now
where the time goes in v2:
time: 82.6 us; the launch traced here: 82.3 us
  Pallas kernels  77.6 us (94%)
  local copies, waits for them, and re-layouts  4.7 us (6%)
    pallas_call x1, Pallas kernels, fused(): pl.pallas_call(functools.partial(kernel, ep_count, tp_count, cap), out_sh...  77.6 us
    unnamed x3, local copies, waits for them, and re-layouts  4.7 us

profile of v2, /device:TPU:0, one launch (start us, length us, event | category | flops | bytes accessed | tf_op | source)
XLA Modules:
  0.0 82.3 jit_solution(2030950918472966922)
XLA Ops:
  0.0 1.4 %copy.8.ids_ref = s32[128,2]{1,0:T(8,128)} copy(s32[128,2]{0,1:T(2,128)} %param.9) | data formatting | bytes 2048 | tf_op args[2]
  1.4 1.4 %copy.9.wts_ref = f32[128,2]{1,0:T(8,128)} copy(f32[128,2]{0,1:T(2,128)} %param.10) | data formatting | bytes 2048 | tf_op args[3]
  2.8 77.6 %shard_map.73 = bf16[128,2048]{1,0:T(8,128)(2,1)} custom-call(bf16[128,2048]{1,0:T(8,128)(2,1)} %x_ref.1, f32[1,2048]{1,0:T(1,128)} %bitcast.1, s32[128,2]{1,0:T(8,128)} %copy.8.ids_ref, f32[128,2]{1,0:T(8,128)} %copy.9.wts_ref, bf16[1,2048,512]{2,1,0:T(8,128)(2,1)} %wg_hbm.1, bf16[1,2048,512]{2,1,0:T(8,128)(2,1)} %wu_hbm.1, bf16[1,512,2048]{2,1,0:T(8,128)(2,1)} %wd_hbm.1), custom_call_target="tpu_custom_call" | custom-call | tf_op jit(solution)/shard_map/pallas_call | solution.py:367
  80.5 1.9 %copy.11 = bf16[128,2048]{1,0:T(8,128)(2,1)} copy(bf16[128,2048]{1,0:T(8,128)(2,1)} %shard_map.73) | data formatting | bytes 1048576

commit v3 on v2

--- a/solution.py
+++ b/solution.py
@@ -51,12 +51,13 @@
     return index
 
 
-PIECES = 2
+PIECES = 4
 
 
 def kernel(
     ep_count, tp_count, cap,
-    x_ref, gain_ref, ids_ref, wts_ref, wg_hbm, wu_hbm, wd_hbm, out_ref,
+    x_hbm, gain_ref, ids_ref, wts_ref, wg_hbm, wu_hbm, wd_hbm, out_hbm,
+    x_ref, out_ref, io_sem,
     normed, meta, share_hi, share_lo, nsend, nrecv, nres, nback,
     rblock, rmeta, rpick, rshare_hi, rshare_lo, fsend, frecv, fres, rback, rsend, farback,
     wg, wu, wd, acc,
@@ -66,7 +67,7 @@
     ep, tp, grp = lax.axis_index("ep"), lax.axis_index("tp"), lax.axis_index("grp")
     rows, width = x_ref.shape
     part_w = width // PIECES
-    top = ids_ref.shape[1]
+    top = ids_ref.shape[0]
     experts = ep_count * tp_count
     near = 2 * tp_count
     me = ep * tp_count + tp
@@ -85,11 +86,20 @@
         )
 
     barrier = pltpu.get_barrier_semaphore()
-    for g in range(1, experts):
-        pl.semaphore_signal(
-            barrier, inc=1, device_id=at(flipped(ep, g // tp_count), g % tp_count),
-            device_id_type=MESH,
-        )
+
+    def greet(target):
+        pl.semaphore_signal(barrier, inc=1, device_id=target, device_id_type=MESH)
+
+    greet(at(flipped(ep, 2), 0))
+
+    @pl.when(is_boundary)
+    def _():
+        greet(at(flipped(ep, 3), 0))
+
+    for g in range(near - 1, 0, -1):
+        greet(at(flipped(ep, g // tp_count), g % tp_count))
+    fetch = pltpu.make_async_copy(x_hbm, x_ref, io_sem.at[0])
+    fetch.start()
     loads = [
         pltpu.make_async_copy(src.at[0], dst, w_sem.at[i])
         for i, (src, dst) in enumerate(((wg_hbm, wg), (wu_hbm, wu), (wd_hbm, wd)))
@@ -105,6 +115,12 @@
     ]
     meta_copy = remote(meta, rmeta.at[wave_of_me], meta_s.at[0], meta_r.at[wave_of_me],
                        at(other_relay, 0))
+    stores = [
+        pltpu.make_async_copy(
+            out_ref.at[:, pl.ds(c * part_w, part_w)], out_hbm.at[:, pl.ds(c * part_w, part_w)],
+            io_sem.at[1 + c])
+        for c in range(PIECES)
+    ]
     near_out = [
         remote(nsend.at[g], nrecv.at[g], near_s.at[g], near_r.at[g],
                at(planes[g // tp_count], g % tp_count))
@@ -130,6 +146,24 @@
             final[v, c] = remote(rsend.at[v, c], farback.at[c], final_s.at[v, c], final_r.at[c],
                                  at(flipped(ep, 3 - v), 0))
 
+    down = lax.broadcasted_iota(jnp.int32, (rows, rows), 0)
+    across = lax.broadcasted_iota(jnp.int32, (rows, rows), 1)
+
+    expert_of = lax.broadcasted_iota(jnp.int32, (experts, rows), 0) ^ me
+    ids, wts = ids_ref[...], wts_ref[...]
+    named = jnp.zeros((experts, rows), jnp.float32)
+    weight = jnp.zeros((experts, rows), jnp.float32)
+    for k in range(top):
+        match = ids[k:k + 1] == expert_of
+        named = named + jnp.where(match, 1.0, 0.0)
+        weight = weight + jnp.where(match, wts[k:k + 1], 0.0)
+    earlier = jnp.where(down < across, 1.0, 0.0).astype(jnp.bfloat16)
+    rank = jnp.dot(named.astype(jnp.bfloat16), earlier, preferred_element_type=jnp.float32)
+    rank = jnp.where(named > 0.5, rank, -1.0)
+    meta[0:near] = rank[near:]
+    meta[near:] = weight[near:]
+
+    fetch.wait()
     values = x_ref[...].astype(jnp.float32)
     rows_normed = (
         values
@@ -139,26 +173,6 @@
     for c in range(PIECES):
         normed[c] = rows_normed[:, c * part_w:(c + 1) * part_w]
 
-    down = lax.broadcasted_iota(jnp.int32, (rows, rows), 0)
-    across = lax.broadcasted_iota(jnp.int32, (rows, rows), 1)
-
-    def as_row(column):
-        return jnp.sum(jnp.where(down == across, column, 0), axis=0, keepdims=True)
-
-    expert_of = lax.broadcasted_iota(jnp.int32, (experts, rows), 0) ^ me
-    ids, wts = ids_ref[...], wts_ref[...]
-    named = jnp.zeros((experts, rows), jnp.float32)
-    weight = jnp.zeros((experts, rows), jnp.float32)
-    for k in range(top):
-        match = as_row(ids[:, k:k + 1]) == expert_of
-        named = named + jnp.where(match, 1.0, 0.0)
-        weight = weight + jnp.where(match, as_row(wts[:, k:k + 1]), 0.0)
-    earlier = jnp.where(down < across, 1.0, 0.0).astype(jnp.bfloat16)
-    rank = jnp.dot(named.astype(jnp.bfloat16), earlier, preferred_element_type=jnp.float32)
-    rank = jnp.where(named > 0.5, rank, -1.0)
-    meta[0:near] = rank[near:]
-    meta[near:] = weight[near:]
-
     def onehots(rank, weight):
         slot = lax.broadcasted_iota(jnp.int32, (near, cap, rows), 1).astype(jnp.float32)
         taken = rank[:, None, :] == slot
@@ -167,7 +181,7 @@
         high = share.astype(jnp.bfloat16)
         return pick, high, (share - high.astype(jnp.float32)).astype(jnp.bfloat16)
 
-    pl.semaphore_wait(barrier, experts - 1)
+    pl.semaphore_wait(barrier, near + boundary)
 
     @pl.when(is_boundary)
     def _():
@@ -223,9 +237,9 @@
                 nres[base + j] = result[j]
             else:
                 nback[0] = result[0]
-        for j in range(tp_count):
-            if p or j:
-                near_ret[base + j].start()
+        if p == 0:
+            for j in range(1, tp_count):
+                near_ret[j].start()
 
     def relay_out(v, c):
         @pl.when(is_boundary)
@@ -301,19 +315,32 @@
 
     for load in loads:
         load.wait()
+    def return_near(cond, js):
+        @pl.when(cond)
+        def _():
+            for j in js:
+                near_ret[tp_count + j].start()
+
+    def return_near(cond, js):
+        @pl.when(cond)
+        def _():
+            for j in js:
+                near_ret[tp_count + j].start()
+
     expert_near(0)
     relay_out(0, 0)
     expert_near(1)
+    return_near(is_end, range(tp_count))
     for c in range(1, PIECES):
         relay_out(0, c)
-    relay_out(1, 0)
     expert_far(0)
-    for c in range(1, PIECES):
+    for c in range(PIECES):
         relay_out(1, c)
-    relay_back(0, 0)
+    return_near(is_boundary, range(tp_count))
+    for c in range(PIECES):
+        relay_back(0, c)
     expert_far(1)
-    for c in range(1, PIECES):
-        relay_back(0, c)
+    pass
 
     for g in range(1, near):
         near_ret[g].wait_recv()
@@ -324,7 +351,10 @@
         final[0, c].wait_recv()
         part = acc[:, c * part_w:(c + 1) * part_w] + farback[c].astype(jnp.float32)
         out_ref[:, c * part_w:(c + 1) * part_w] = part.astype(out_ref.dtype)
-
+        stores[c].start()
+
+    for store in stores:
+        store.wait()
     meta_copy.wait_send()
     for copy in dense + near_out[1:] + near_ret[1:]:
         copy.wait_send()
@@ -367,9 +397,10 @@
     return pl.pallas_call(
         functools.partial(kernel, ep_count, tp_count, cap),
         out_shape=jax.ShapeDtypeStruct((rows, width), tokens.dtype),
-        in_specs=[vmem] * 4 + [hbm] * 3,
-        out_specs=vmem,
+        in_specs=[hbm] + [vmem] * 3 + [hbm] * 3,
+        out_specs=hbm,
         scratch_shapes=[
+            b16(rows, width), b16(rows, width), sems(1 + PIECES),
             b16(PIECES, rows, part_w), pltpu.VMEM((2 * near, rows), jnp.float32),
             b16(near * cap, rows), b16(near * cap, rows),
             *[b16(near, cap, width)] * 4,
@@ -391,7 +422,7 @@
         compiler_params=pltpu.CompilerParams(
             collective_id=0, has_side_effects=True, vmem_limit_bytes=56 * 1024 * 1024
         ),
-    )(tokens, norm_gain.reshape(1, width), route_ids, route_weights, w_gate, w_up, w_down)
+    )(tokens, norm_gain.reshape(1, width), route_ids.T, route_weights.T, w_gate, w_up, w_down)
 
 
 def solution(mesh):

time: 82.6 us -> 73.8 us (0.89)
  Pallas kernels: 77.6 us -> 71.7 us
  local copies, waits for them, and re-layouts: 4.7 us -> 1.88 us
    pallas_call x1, Pallas kernels: 77.6 us -> 71.7 us  [fused(): pl.pallas_call(functools.partial(kernel, ep_count, tp_count, cap), out_sh...]
    unnamed x3 -> x1, local copies, waits for them, and re-layouts: 4.7 us -> 1.88 us
where the time goes in v3:
time: 73.8 us; the launch traced here: 73.6 us
  Pallas kernels  71.7 us (97%)
  local copies, waits for them, and re-layouts  1.88 us (3%)
    pallas_call x1, Pallas kernels, fused(): pl.pallas_call(functools.partial(kernel, ep_count, tp_count, cap), out_sh...  71.7 us
    unnamed x1, local copies, waits for them, and re-layouts  1.88 us

profile of v3, /device:TPU:0, one launch (start us, length us, event | category | flops | bytes accessed | tf_op | source)
XLA Modules:
  0.0 73.6 jit_solution(17049074544683762942)
XLA Ops:
  0.0 71.7 %shard_map.73 = bf16[128,2048]{1,0:T(8,128)(2,1)} custom-call(bf16[128,2048]{1,0:T(8,128)(2,1)} %x_hbm.1, f32[1,2048]{1,0:T(1,128)} %bitcast.3, s32[2,128]{1,0:T(2,128)} %bitcast.4, f32[2,128]{1,0:T(2,128)} %bitcast.5, bf16[1,2048,512]{2,1,0:T(8,128)(2,1)} %wg_hbm.1, bf16[1,2048,512]{2,1,0:T(8,128)(2,1)} %wu_hbm.1, bf16[1,512,2048]{2,1,0:T(8,128)(2,1)} %wd_hbm.1), custom_call_target="tpu_custom_call" | custom-call | tf_op jit(solution)/shard_map/pallas_call | solution.py:397
  71.7 1.9 %copy.9 = bf16[128,2048]{1,0:T(8,128)(2,1)} copy(bf16[128,2048]{1,0:T(8,128)(2,1)} %shard_map.73) | data formatting | bytes 1048576
